TPU v7x, 32 devices: a whole 2x2x4 slice. The times are simulated.
32 devices in a mesh: grp: 2 (over y), sp: 4 (over z), tp: 4 (over x, core).
Axes of the slice: x: 2, y: 2, z: 4, core: 2. Of those that a mesh axis runs over, the one named last changes fastest.
Arguments:
- tokens: bfloat16 [4096, 2048], P(('grp', 'sp')), parts along dimension 0, may hold values from -6 to 6
- fresh_token_input: bfloat16 [4096], P('grp'), parts along dimension 0, may hold values from -6 to 6
- value_matrix: bfloat16 [2048, 2048], P(None, 'tp'), may hold values from -0.125 to 0.125
- write_matrix: bfloat16 [2048, 1024], P(None, 'tp'), may hold values from -0.125 to 0.125
- read_matrix: bfloat16 [2048, 1024], P(None, 'tp'), may hold values from -0.125 to 0.125
- gate_matrix: bfloat16 [2048, 2048], P(None, 'tp'), may hold values from -0.125 to 0.125
- step_matrix: bfloat16 [2048, 32], replicated, may hold values from -0.125 to 0.125
- value_filter_taps: bfloat16 [4, 2048], replicated, may hold values from -3 to 3
- write_filter_taps: bfloat16 [4, 1024], replicated, may hold values from -3 to 3
- read_filter_taps: bfloat16 [4, 1024], replicated, may hold values from -3 to 3
- head_log_decay: float32 [32], replicated
- step_offset_bias: float32 [32], replicated, may hold values from -3.5 to -2.5
- decay_spike: float32 [4096, 32], P(('grp', 'sp'), 'tp'), parts along dimension 0, may hold values from -3 to 0, as said below
- bypass_scale: float32 [32], replicated, may hold values from 0.5 to 2
- group_norm_scale: float32 [2048], replicated, may hold values from 0.1 to 1.9
Outputs:
- prompt_out: bfloat16 [4096, 2048], P(('grp', 'sp'), 'tp'), parts along dimension 0
- state_cache: bfloat16 [256, 2048], P(('grp', 'sp'), 'tp'), parts along dimension 0
- step_out: bfloat16 [1024, 4], P(('grp', 'tp'), 'sp'), parts along dimension 0
There are 2 independent parts, one for each index of `grp`. A program takes and returns all parts, laid end to end along the dimension named above; an argument that names none is the same for every part. Nothing has to cross between parts.
Inputs may be any that keep to these rules, and one draw needn't show every extreme that they name: `decay_spike`: never positive.
All inputs are finite; a program needn't handle non-finite values.
Results may differ from a plain program's by a relative error of at most 0.023.
Values may be sent and summed in bfloat16 or wider, within the bound.
A program may use at most 64 MiB of HBM per device.

v0:
```python
import jax
import jax.numpy as jnp
from jax import lax
from jax.sharding import PartitionSpec as P

HEAD = 64
STATE = 128
CONV = 4
BLOCK = 128
epsilon = 1e-06


def passed_along(block, axis, distance):
    devices = range(lax.axis_size(axis))
    route = [(i - distance, i) for i in devices if i - distance in devices]
    return lax.ppermute(block, axis, route)


def from_root(value, axis, source):
    kept = jnp.where(lax.axis_index(axis) == source, value, 0).astype(value.dtype)
    return lax.psum(kept, axis)


def project(operand, weights):
    return jnp.dot(operand, weights, preferred_element_type=jnp.float32).astype(jnp.bfloat16)


def apply_taps(previous, current, tap_weights):
    joined = jnp.concatenate([previous, current], axis=0).astype(jnp.float32)
    length = current.shape[0]
    summed = jnp.zeros(current.shape, jnp.float32)
    for offset in range(CONV):
        summed = summed + tap_weights[offset].astype(jnp.float32) * joined[offset : offset + length]
    return summed


def group_norm(gated_rows, groups):
    shaped = gated_rows.reshape(gated_rows.shape[:-1] + (groups, -1))
    normed = shaped * lax.rsqrt(jnp.mean(shaped * shaped, axis=-1, keepdims=True) + epsilon)
    return normed.reshape(gated_rows.shape)


def read_new(cached, stored_portion, read_part, new_decay, step_now, value_now):
    states = cached.astype(jnp.float32).reshape((cached.shape[0],) + value_now.shape)
    updated = (
        new_decay[None, :, :, None] * states
        + step_now[None, :, :, None] * stored_portion.T[:, :, None, None] * value_now[None]
    )
    return jnp.einsum("gn,ngep->gep", read_part, updated, precision=lax.Precision.HIGHEST)


def on_device(
    tokens,
    fresh_token_input,
    value_matrix,
    write_matrix,
    read_matrix,
    gate_matrix,
    step_matrix,
    value_filter_taps,
    write_filter_taps,
    read_filter_taps,
    head_log_decay,
    step_offset_bias,
    decay_spike,
    bypass_scale,
    group_norm_scale,
):
    head_rank = lax.axis_index("tp")
    sequence_rank = lax.axis_index("sp")
    sequence_count = lax.axis_size("sp")
    channels = value_matrix.shape[1]
    head_count = channels // HEAD
    map_width = write_matrix.shape[1]
    group_count = map_width // STATE
    per_group = head_count // group_count
    row_count = tokens.shape[0]
    head_start = head_rank * head_count
    local_count = STATE // sequence_count
    own_step = lax.dynamic_slice_in_dim(step_matrix, head_start, head_count, 1)
    own_value_taps = lax.dynamic_slice_in_dim(value_filter_taps, head_rank * channels, channels, 1)
    own_write_taps = lax.dynamic_slice_in_dim(
        write_filter_taps, head_rank * map_width, map_width, 1
    )
    own_read_taps = lax.dynamic_slice_in_dim(read_filter_taps, head_rank * map_width, map_width, 1)
    head_decay_rates = jnp.exp(lax.dynamic_slice_in_dim(head_log_decay, head_start, head_count, 0))
    own_bias = lax.dynamic_slice_in_dim(step_offset_bias, head_start, head_count, 0)
    own_skip = lax.dynamic_slice_in_dim(bypass_scale, head_start, head_count, 0)
    own_gain = lax.dynamic_slice_in_dim(group_norm_scale, head_rank * channels, channels, 0)
    value_rows = project(tokens, value_matrix)
    write_rows = project(tokens, write_matrix)
    read_rows = project(tokens, read_matrix)
    gate_rows = project(tokens, gate_matrix)
    step_raw = jnp.dot(tokens, own_step, preferred_element_type=jnp.float32)
    edge = row_count - (CONV - 1)
    tail_rows = (value_rows[edge:], write_rows[edge:], read_rows[edge:])
    before = passed_along((tail_rows[0], tail_rows[1], tail_rows[2]), "sp", 1)
    ending = (
        from_root(tail_rows[0], "sp", sequence_count - 1),
        from_root(tail_rows[1], "sp", sequence_count - 1),
        from_root(tail_rows[2], "sp", sequence_count - 1),
    )
    values = jax.nn.silu(apply_taps(before[0], value_rows, own_value_taps)).astype(jnp.bfloat16)
    writes = jax.nn.silu(apply_taps(before[1], write_rows, own_write_taps)).astype(jnp.bfloat16)
    reads = jax.nn.silu(apply_taps(before[2], read_rows, own_read_taps)).astype(jnp.bfloat16)
    step_length = jax.nn.softplus(step_raw + own_bias)
    log_decay_value = decay_spike - step_length * head_decay_rates
    blocks = row_count // BLOCK
    block_values = values.reshape(blocks, BLOCK, group_count, per_group, HEAD)
    block_writes = writes.reshape(blocks, BLOCK, group_count, STATE)
    block_reads = reads.reshape(blocks, BLOCK, group_count, STATE)
    block_steps = step_length.reshape(blocks, BLOCK, group_count, per_group)
    cumulative = jnp.cumsum(log_decay_value.reshape(blocks, BLOCK, group_count, per_group), axis=1)
    block_end = cumulative[:, -1]
    scaled = (
        (jnp.exp(block_end[:, None] - cumulative) * block_steps)[..., None]
        * block_values.astype(jnp.float32)
    ).astype(jnp.bfloat16)
    block_states = jnp.einsum(
        "bsgn,bsgep->bngep", block_writes, scaled, preferred_element_type=jnp.float32
    )
    running = jnp.zeros((STATE, group_count, per_group, HEAD), jnp.float32)
    inside = []
    for block_index in range(blocks):
        inside.append(running)
        running = (
            jnp.exp(block_end[block_index])[None, :, :, None] * running + block_states[block_index]
        )
    local_states = jnp.stack(inside)
    shard_fading_factor = jnp.sum(block_end, axis=0)
    before_block = jnp.cumsum(block_end, axis=0) - block_end
    decay_table = lax.all_gather(shard_fading_factor[None], "sp", axis=0, tiled=True)
    inclusive = jnp.cumsum(decay_table, axis=0)
    exclusive = inclusive - decay_table
    total_decay = inclusive[-1]
    row_pieces = lax.all_to_all(running[None], "sp", split_axis=1, concat_axis=0, tiled=True)
    ranks = jnp.arange(sequence_count)
    below = (ranks[None, :] < ranks[:, None])[:, :, None, None]
    prefix_weight = jnp.exp(jnp.where(below, exclusive[:, None] - inclusive[None, :], -jnp.inf))
    prefix_rows = jnp.einsum(
        "jkge,kngep->jngep", prefix_weight, row_pieces, precision=lax.Precision.HIGHEST
    )
    final_weight = jnp.exp(total_decay[None] - inclusive)
    final_rows = jnp.einsum(
        "kge,kngep->ngep", final_weight, row_pieces, precision=lax.Precision.HIGHEST
    )
    earlier_state = lax.all_to_all(prefix_rows, "sp", split_axis=0, concat_axis=1, tiled=True)[0]
    scores = jnp.einsum(
        "blgn,bsgn->bgls", block_reads, block_writes, preferred_element_type=jnp.float32
    )
    cum_heads = jnp.transpose(cumulative, (0, 2, 3, 1))
    decay_gaps = cum_heads[..., :, None] - cum_heads[..., None, :]
    step_heads = jnp.transpose(block_steps, (0, 2, 3, 1))
    causal = jnp.tril(jnp.ones((BLOCK, BLOCK), bool))
    mixing = (
        scores[:, :, None]
        * jnp.exp(jnp.where(causal, decay_gaps, -jnp.inf))
        * step_heads[..., None, :]
    ).astype(jnp.bfloat16)
    inner_part = jnp.einsum(
        "bgels,bsgep->blgep", mixing, block_values, preferred_element_type=jnp.float32
    )
    entering = jnp.exp(before_block)[:, None, :, :, None] * earlier_state[None] + local_states
    carried_part = jnp.exp(cumulative)[..., None] * jnp.einsum(
        "blgn,bngep->blgep",
        block_reads.astype(jnp.float32),
        entering,
        precision=lax.Precision.HIGHEST,
    )
    mixed_rows = (inner_part + carried_part).reshape(row_count, head_count, HEAD) + own_skip[
        None, :, None
    ] * values.astype(jnp.float32).reshape(row_count, head_count, HEAD)
    gated_rows = mixed_rows.reshape(row_count, channels) * jax.nn.silu(
        gate_rows.astype(jnp.float32)
    )
    prompt_out = (group_norm(gated_rows, group_count) * own_gain).astype(jnp.bfloat16)
    new_row = fresh_token_input[None]
    new_value = project(new_row, value_matrix)
    new_write = project(new_row, write_matrix)
    new_read = project(new_row, read_matrix)
    new_gate = project(new_row, gate_matrix)
    new_step = jax.nn.softplus(
        jnp.dot(new_row, own_step, preferred_element_type=jnp.float32)[0] + own_bias
    )
    new_values = jax.nn.silu(apply_taps(ending[0], new_value, own_value_taps)).astype(jnp.bfloat16)
    latest_stores = jax.nn.silu(apply_taps(ending[1], new_write, own_write_taps)).astype(
        jnp.bfloat16
    )
    new_reads = jax.nn.silu(apply_taps(ending[2], new_read, own_read_taps)).astype(jnp.bfloat16)
    value_now = new_values.astype(jnp.float32).reshape(group_count, per_group, HEAD)
    write_now = latest_stores.astype(jnp.float32).reshape(group_count, STATE)
    read_now = new_reads.astype(jnp.float32).reshape(group_count, STATE)
    new_decay = jnp.exp(-new_step * head_decay_rates).reshape(group_count, per_group)
    step_now = new_step.reshape(group_count, per_group)
    row_start = sequence_rank * local_count
    cache_rows = final_rows.reshape(local_count, channels).astype(jnp.bfloat16)
    stored_portion = lax.dynamic_slice_in_dim(write_now, row_start, local_count, 1)
    read_part = lax.dynamic_slice_in_dim(read_now, row_start, local_count, 1)
    partial_value = read_new(cache_rows, stored_portion, read_part, new_decay, step_now, value_now)
    reading = lax.psum(partial_value, "sp")
    new_mixed = reading + own_skip.reshape(group_count, per_group)[:, :, None] * value_now
    new_gated = new_mixed.reshape(1, channels) * jax.nn.silu(new_gate.astype(jnp.float32))
    step_whole = (group_norm(new_gated, group_count) * own_gain).astype(jnp.bfloat16)[0]
    step_table = step_whole.reshape(channels // sequence_count, sequence_count)
    step_out = lax.dynamic_slice_in_dim(step_table, sequence_rank, 1, 1)
    return (prompt_out, cache_rows, step_out)


def solution(mesh):
    placed = (
        P(("grp", "sp"), None),
        P("grp"),
        P(None, "tp"),
        P(None, "tp"),
        P(None, "tp"),
        P(None, "tp"),
        P(),
        P(),
        P(),
        P(),
        P(),
        P(),
        P(("grp", "sp"), "tp"),
        P(),
        P(),
    )
    return jax.shard_map(
        on_device,
        mesh=mesh,
        in_specs=placed,
        out_specs=(P(("grp", "sp"), "tp"), P(("grp", "sp"), "tp"), P(("grp", "tp"), "sp")),
        check_vma=False,
    )
```

profile of v0, /device:TPU:0, one launch (start us, length us, event | category | flops | bytes accessed | tf_op | source)
XLA Modules:
  0.0 126.4 jit_solution(4960432107386798171)
XLA Ops:
  0.7 1.6 %copy-done = bf16[512,2048]{1,0:T(8,128)(2,1)S(1)} copy-done((bf16[512,2048]{1,0:T(8,128)(2,1)S(1)}, bf16[512,2048]{1,0:T(8,128)(2,1)}, u32[]{:S(2)}) %copy-start) | copy-done | bytes 2097176
  2.2 1.9 %convolution_convert_fusion.2 = bf16[512,256]{1,0:T(8,128)(2,1)S(1)} fusion(bf16[512,2048]{1,0:T(8,128)(2,1)S(1)} %copy-done, bf16[2048,256]{1,0:T(8,128)(2,1)} %param.18), kind=kOutput, calls=%fused_computation.11 | convolution fusion | flops 537001984 | bytes 3407872 | tf_op jit(solution)/shard_map/dot_general | solution.py:25
  4.7 5.7 %collective-permute-start.2 = (bf16[3,256]{1,0:T(4,128)(2,1)}, bf16[3,256]{1,0:T(4,128)(2,1)}, u32[]{:S(2)}, u32[]{:S(2)}) collective-permute-start(bf16[3,256]{1,0:T(4,128)(2,1)} %get-tuple-element.57), channel_id=1, source_target_pairs={{0,4},{4,8},{8,12},{1,5},{5,9},{9,13},{2,6},{6,10},{10,14},{3,7},{... | collective-permute-start | bytes 4616 | tf_op jit(solution)/shard_map/ppermute | solution.py:16
  10.4 0.7 convolution_convert_fusion.3
  11.8 3.6 %collective-permute-start.1 = (bf16[3,256]{1,0:T(4,128)(2,1)}, bf16[3,256]{1,0:T(4,128)(2,1)}, u32[]{:S(2)}, u32[]{:S(2)}) collective-permute-start(bf16[3,256]{1,0:T(4,128)(2,1)} %get-tuple-element.54), channel_id=1, source_target_pairs={{0,4},{4,8},{8,12},{1,5},{5,9},{9,13},{2,6},{6,10},{10,14},{3,7},{... | collective-permute-start | bytes 4616 | tf_op jit(solution)/shard_map/ppermute | solution.py:16
  15.4 1.3 convolution_convert_fusion.1
  16.7 0.8 copy-done.8
  18.1 3.5 %collective-permute-start = (bf16[3,512]{1,0:T(4,128)(2,1)}, bf16[3,512]{1,0:T(4,128)(2,1)}, u32[]{:S(2)}, u32[]{:S(2)}) collective-permute-start(bf16[3,512]{1,0:T(4,128)(2,1)} %get-tuple-element.52), channel_id=1, source_target_pairs={{0,4},{4,8},{8,12},{1,5},{5,9},{9,13},{2,6},{6,10},{10,14},{3,7},{... | collective-permute-start | bytes 9224 | tf_op jit(solution)/shard_map/ppermute | solution.py:16
  22.4 1.5 %fusion.96 = f32[1,256]{1,0:T(1,128)S(1)} fusion(bf16[2048,1]{0,1:T(2,128)(2,1)S(1)} %reshape.251, bf16[2048,256]{1,0:T(8,128)(2,1)} %param.19), kind=kOutput, calls=%fused_computation.194 | convolution fusion | flops 1048576 | bytes 1053696 | tf_op jit(solution)/shard_map/dot_general | solution.py:25
  27.1 2.0 %fusion.99 = f32[1,512]{1,0:T(1,128)S(1)} fusion(bf16[2048,1]{0,1:T(2,128)(2,1)S(1)} %reshape.251, bf16[2048,512]{1,0:T(8,128)(2,1)} %param.20), kind=kOutput, calls=%fused_computation.197 | convolution fusion | flops 2097152 | bytes 2103296 | tf_op jit(solution)/shard_map/dot_general | solution.py:25
  29.1 7.6 %all-gather.1 = f32[4,2,4]{2,1,0:T(2,128)S(1)} all-gather(f32[1,2,4]{2,1,0:T(2,128)S(1)} %bitcast.152), channel_id=2, replica_groups=mesh['grp'=2,'sp'=4,'tp'=4] {'sp'}, dimensions={0}, use_global_device_ids=true | all-gather | bytes 160 | tf_op jit(solution)/shard_map/all_gather | solution.py:132
  36.7 10.5 %all-reduce = (bf16[3,512]{1,0:T(4,128)(2,1)S(1)}, bf16[3,256]{1,0:T(4,128)(2,1)S(1)}, bf16[3,256]{1,0:T(4,128)(2,1)S(1)}) all-reduce(bf16[3,512]{1,0:T(4,128)(2,1)S(1)} %get-tuple-element.53, bf16[3,256]{1,0:T(4,128)(2,1)S(1)} %get-tuple-element.56, ...), channel_id=1, replica_groups=mesh['grp'=2,'sp'=4,'tp'=4] {'sp'}, use_global_device_ids=true, to_apply=%region_7.8 | all-reduce | flops 3072 | bytes 12288 | tf_op jit(solution)/shard_map/psum | solution.py:21
  48.1 1.0 copy.149
  49.2 0.7 convert_reduce_fusion.1
  49.9 2.4 %fusion.90 = (f32[4,128,2,4]{3,2,1,0:T(2,128)}, f32[4,128,2,4]{3,2,1,0:T(2,128)S(1)}) fusion(f32[4,128,2,4]{3,2,1,0:T(2,128)S(1)} %fusion.94, f32[4,128,2,4]{3,2,1,0:T(2,128)} %copy.149, f32[4,2,4]{2,1,0:T(2,128)S(1)} %get-tuple-element.47), kind=kLoop, calls=%fused_computation.187 | loop fusion | flops 8192 | bytes 65664 | tf_op jit(solution)/shard_map/exp | solution.py:164
  52.4 0.7 convert_reduce_fusion
  53.7 0.7 dynamic_slice.39
  55.9 1.3 %mul.529 = f32[2,4]{1,0:T(2,128)} reshape(f32[8]{0:T(128)} %get-tuple-element.28) | data formatting | bytes 64 | tf_op jit(solution)/shard_map/mul | solution.py:46
  57.6 1.3 %copy.148 = f32[4,128,2,4]{1,3,2,0:T(4,128)S(1)} copy(f32[4,128,2,4]{3,2,1,0:T(2,128)} %get-tuple-element.44) | data formatting | bytes 32768 | tf_op jit(solution)/shard_map/exp | solution.py:164
  59.7 0.7 maximum_convert_fusion.2
  60.5 1.0 multiply_convert_fusion.5
  61.5 0.8 maximum_convert_fusion.1
  62.8 0.8 maximum_convert_fusion
  63.6 1.3 %multiply_convert_fusion.4 = bf16[512,512]{1,0:T(8,128)(2,1)S(1)} fusion(f32[515,512]{1,0:T(8,128)S(1)} %maximum_convert_fusion, f32[512]{0:T(512)} %bitcast.141, f32[512]{0:T(512)} %bitcast.140, f32[512]{0:T(512)S(1)} %bitcast.139, f32[512]{0:T(512)S(1)} %bitcast.138), kind=kLoop, calls=%fused_computation.44 | loop fusion | flops 3145728 | bytes 4726784 | tf_op jit(solution)/shard_map/convert_element_type | solution.py:103
  65.0 1.0 copy.140
  66.0 2.0 %reshape.229 = bf16[4,128,2,4,64]{1,0,4,3,2:T(4,128)(2,1)} reshape(bf16[512,512]{0,1:T(8,128)(2,1)} %copy.140) | data formatting | bytes 1048576 | tf_op jit(solution)/shard_map/reshape | solution.py:109
  68.0 1.3 multiply_convert_fusion.3
  69.5 1.0 slice_add_fusion
  70.8 1.2 reshape.274
  72.0 3.6 %all-to-all-start = ((f32[4,1,16384]{2,1,0:T(1,128)}), f32[4,1,16384]{2,1,0:T(1,128)S(1)}, u32[]{:S(2)}, u32[]{:S(2)}) async-start(f32[4,1,16384]{2,1,0:T(1,128)} %reshape.274), calls=%async_computation | async-start | bytes 524288 | tf_op jit(solution)/shard_map/all_to_all | solution.py:136
  75.9 3.0 %convolution_bitcast_fusion.2 = f32[4,128,2,4,64]{1,4,3,2,0:T(8,128)} fusion(f32[4,2,4,128]{3,2,1,0:T(4,128)S(1)} %copy.146, f32[4,2,4,128]{3,2,1,0:T(4,128)S(1)} %copy.144, f32[4,2,128,128]{3,2,1,0:T(8,128)S(1)} %fusion.40, pred[128,128]{1,0:T(8,128)(4,1)S(1)} %iota_compare_fusion, bf16[4,128,2,4,64]{1,0,4,3,2:T(4,128)(2,1)} %reshape.229), kind=kOutput, calls=%fused_computation.5 | convolution fusion | flops 69730304 | bytes 2146304 | tf_op jit(solution)/shard_map/bgels,bsgep->blgep/dot_general | solution.py:160
  78.8 3.3 %all-to-all-done = f32[4,1,16384]{2,1,0:T(1,128)S(1)} async-done(((f32[4,1,16384]{2,1,0:T(1,128)}), f32[4,1,16384]{2,1,0:T(1,128)S(1)}, u32[]{:S(2)}, u32[]{:S(2)}) %all-to-all-start) | async-done | bytes 262176 | tf_op jit(solution)/shard_map/all_to_all | solution.py:136
  82.7 1.3 %reduce.9 = f32[4,16384]{1,0:T(4,128)S(1)} reduce(f32[4,1,16384]{2,1,0:T(1,128)S(1)} %all-to-all-done, f32[]{:T(128)} %broadcast.118), dimensions={1}, to_apply=%all_to_all.6.reduce_sub_computation | reduce | bytes 524292 | tf_op jit(solution)/shard_map/all_to_all | solution.py:136
  84.4 1.3 %fusion.35 = bf16[2,4,1,32,64]{4,2,3,1,0:T(2,128)(2,1)S(1)} fusion(f32[4,2,4,1,1]{0,3,4,2,1:T(1,128)S(1)} %copy.173, f32[4,32,2,4,64]{4,3,2,1,0:T(4,128)S(1)} %bitcast.123), kind=kOutput, calls=%fused_computation.69 | convolution fusion | flops 786432 | bytes 295040 | tf_op jit(solution)/shard_map/kge,kngep->ngep/dot_general | solution.py:144
  85.7 1.3 %convolution_bitcast_fusion.3 = f32[4,32,2,4,64]{4,0,1,3,2:T(4,128)S(1)} fusion(f32[4,32,2,4,64]{4,3,2,1,0:T(4,128)S(1)} %bitcast.124, f32[4,2,4]{0,2,1:T(4,128)S(1)} %copy.156, f32[4,2,4]{0,2,1:T(4,128)S(1)} %copy.155, pred[4,4]{1,0:T(4,128)(4,1)S(1)} %copy-done.30), kind=kOutput, calls=%fused_computation.10 | convolution fusion | flops 3145984 | bytes 524560 | tf_op jit(solution)/shard_map/jkge,kngep->jngep/dot_general | solution.py:140
  87.1 1.0 reshape.276
  88.1 3.4 %all-to-all-start.1 = ((f32[4,1,16384]{2,1,0:T(1,128)}), f32[4,1,16384]{2,1,0:T(1,128)S(1)}, u32[]{:S(2)}, u32[]{:S(2)}) async-start(f32[4,1,16384]{2,1,0:T(1,128)} %reshape.276), calls=%async_computation.1 | async-start | bytes 524288 | tf_op jit(solution)/shard_map/all_to_all | solution.py:147
  91.9 12.2 %psum.31 = f32[2,4,64]{2,1,0:T(4,128)S(1)} all-reduce(f32[2,4,64]{2,1,0:T(4,128)S(1)} %bitcast.137), channel_id=1, replica_groups=mesh['grp'=2,'sp'=4,'tp'=4] {'sp'}, use_global_device_ids=true, to_apply=%region_8.9 | all-reduce | flops 512 | bytes 4096 | tf_op jit(solution)/shard_map/psum | solution.py:200
  104.5 0.7 convert_element_type.211
  105.3 0.8 multiply_convert_fusion.7
  106.9 1.3 %reduce.10 = f32[4,16384]{1,0:T(4,128)S(1)} reduce(f32[4,1,16384]{2,1,0:T(1,128)S(1)} %all-to-all-done.1, f32[]{:T(128)} %broadcast.118), dimensions={1}, to_apply=%all_to_all.8.reduce_sub_computation | reduce | bytes 524292 | tf_op jit(solution)/shard_map/all_to_all | solution.py:147
  108.5 0.9 copy.160
  109.4 2.3 %fusion.1 = f32[4,128,2,4,64]{1,4,3,2,0:T(8,128)S(1)} fusion(f32[4,128,2,4,64]{1,4,3,2,0:T(8,128)} %convolution_bitcast_fusion.2, f32[1,128,2,4,64]{1,4,3,2,0:T(8,128)} %get-tuple-element.41, f32[1,128,2,4,64]{1,4,3,2,0:T(8,128)} %get-tuple-element.42, f32[1,128,2,4,64]{1,4,3,2,0:T(8,128)} %get-tuple-element.43, f32[4]{0:T(128)S(1)} %copy-done.31, ...), kind=kOutput, calls=%fused_computation.4 | convolution fusion | flops 404488192 | bytes 3424400 | tf_op jit(solution)/shard_map/blgn,bngep->blgep/dot_general | solution.py:164
  111.7 1.8 %copy.184 = f32[4,128,2,4,64]{4,3,2,1,0:T(4,128)} copy(f32[4,128,2,4,64]{1,4,3,2,0:T(8,128)S(1)} %fusion.1) | data formatting | bytes 2097152 | tf_op jit(solution)/shard_map/reshape | solution.py:170
  113.5 3.5 %reshape.263 = f32[512,512]{1,0:T(8,128)} reshape(f32[4,128,2,4,64]{4,3,2,1,0:T(4,128)} %copy.184) | data formatting | bytes 2097152 | tf_op jit(solution)/shard_map/reshape | solution.py:170
  117.0 4.6 %fusion.93 = (f32[512,512]{1,0:T(8,128)}, f32[512,512]{1,0:T(8,128)}) fusion(bf16[512,2048]{1,0:T(8,128)(2,1)S(1)} %copy-done, bf16[2048,512]{1,0:T(8,128)(2,1)} %param.20, f32[512,512]{1,0:T(8,128)} %reshape.263, bf16[512,512]{1,0:T(8,128)(2,1)S(1)} %copy-done.2, f32[512]{0:T(512)S(1)} %copy-done.25), kind=kOutput, calls=%fused_computation.190 | convolution fusion | flops 1076625408 | bytes 7866368 | tf_op jit(solution)/shard_map/dot_general | solution.py:25
  121.7 1.9 %mul.516 = f32[512,2,256]{2,1,0:T(2,128)S(1)} reshape(f32[512,512]{1,0:T(8,128)} %get-tuple-element.63) | data formatting | bytes 2097152 | tf_op jit(solution)/shard_map/mul | solution.py:39
  125.4 1.1 multiply_convert_fusion.2
  (144 shorter events, 16.2 us)
Async XLA Ops:
  0.6 1.6 %copy-start = (bf16[512,2048]{1,0:T(8,128)(2,1)S(1)}, bf16[512,2048]{1,0:T(8,128)(2,1)}, u32[]{:S(2)}) copy-start(bf16[512,2048]{1,0:T(8,128)(2,1)} %param.15) | copy-start | bytes 6291460
  0.6 9.8 %copy-start.6 = (bf16[2048,256]{1,0:T(8,128)(2,1)S(1)}, bf16[2048,256]{1,0:T(8,128)(2,1)}, u32[]{:S(2)}) copy-start(bf16[2048,256]{1,0:T(8,128)(2,1)} %param.19) | copy-start | bytes 3145732
  4.2 11.3 %copy-start.3 = (bf16[2048,512]{1,0:T(8,128)(2,1)S(1)}, bf16[2048,512]{1,0:T(8,128)(2,1)}, u32[]{:S(2)}) copy-start(bf16[2048,512]{1,0:T(8,128)(2,1)} %param.17) | copy-start | bytes 6291460
  4.7 55.0 %collective-permute-start.2 = (bf16[3,256]{1,0:T(4,128)(2,1)}, bf16[3,256]{1,0:T(4,128)(2,1)}, u32[]{:S(2)}, u32[]{:S(2)}) collective-permute-start(bf16[3,256]{1,0:T(4,128)(2,1)} %get-tuple-element.57), channel_id=1, source_target_pairs={{0,4},{4,8},{8,12},{1,5},{5,9},{9,13},{2,6},{6,10},{10,14},{3,7},{... | collective-permute-start | bytes 4616 | tf_op jit(solution)/shard_map/ppermute | solution.py:16
  11.1 0.7 copy-start.10
  11.8 10.3 %copy-start.23 = (bf16[2048]{0:T(1024)(128)(2,1)S(1)}, bf16[2048]{0:T(1024)(128)(2,1)}, u32[]{:S(2)}) copy-start(bf16[2048]{0:T(1024)(128)(2,1)} %param.16) | copy-start | bytes 12292
  11.8 10.3 %copy-start.5 = (bf16[2048,256]{1,0:T(8,128)(2,1)S(1)}, bf16[2048,256]{1,0:T(8,128)(2,1)}, u32[]{:S(2)}) copy-start(bf16[2048,256]{1,0:T(8,128)(2,1)} %param.18) | copy-start | bytes 3145732
  11.8 49.6 %collective-permute-start.1 = (bf16[3,256]{1,0:T(4,128)(2,1)}, bf16[3,256]{1,0:T(4,128)(2,1)}, u32[]{:S(2)}, u32[]{:S(2)}) collective-permute-start(bf16[3,256]{1,0:T(4,128)(2,1)} %get-tuple-element.54), channel_id=1, source_target_pairs={{0,4},{4,8},{8,12},{1,5},{5,9},{9,13},{2,6},{6,10},{10,14},{3,7},{... | collective-permute-start | bytes 4616 | tf_op jit(solution)/shard_map/ppermute | solution.py:16
  16.7 0.8 copy-start.8
  18.1 44.7 %collective-permute-start = (bf16[3,512]{1,0:T(4,128)(2,1)}, bf16[3,512]{1,0:T(4,128)(2,1)}, u32[]{:S(2)}, u32[]{:S(2)}) collective-permute-start(bf16[3,512]{1,0:T(4,128)(2,1)} %get-tuple-element.52), channel_id=1, source_target_pairs={{0,4},{4,8},{8,12},{1,5},{5,9},{9,13},{2,6},{6,10},{10,14},{3,7},{... | collective-permute-start | bytes 9224 | tf_op jit(solution)/shard_map/ppermute | solution.py:16
  21.6 2.3 %copy-start.4 = (bf16[2048,512]{1,0:T(8,128)(2,1)S(1)}, bf16[2048,512]{1,0:T(8,128)(2,1)}, u32[]{:S(2)}) copy-start(bf16[2048,512]{1,0:T(8,128)(2,1)} %param.17) | copy-start | bytes 6291460
  22.1 2.2 %copy-start.33 = (f32[32]{0:T(128)S(1)}, f32[32]{0:T(128)}, u32[]{:S(2)}) copy-start(f32[32]{0:T(128)} %param.26) | copy-start | bytes 388
  22.2 2.3 %copy-start.32 = (f32[32]{0:T(128)S(1)}, f32[32]{0:T(128)}, u32[]{:S(2)}) copy-start(f32[32]{0:T(128)} %param.25) | copy-start | bytes 388
  22.2 3.0 %copy-start.12 = (f32[512,8]{0,1:T(8,128)S(1)}, f32[512,8]{0,1:T(8,128)}, u32[]{:S(2)}) copy-start(f32[512,8]{0,1:T(8,128)} %param.27) | copy-start | bytes 49156
  22.4 2.0 %copy-start.13 = (bf16[2048,32]{0,1:T(8,128)(2,1)S(1)}, bf16[2048,32]{0,1:T(8,128)(2,1)}, u32[]{:S(2)}) copy-start(bf16[2048,32]{0,1:T(8,128)(2,1)} %param.21) | copy-start | bytes 393220
  25.8 21.5 %copy-start.26 = (bf16[4,1024]{1,0:T(4,128)(2,1)S(1)}, bf16[4,1024]{1,0:T(4,128)(2,1)}, u32[]{:S(2)}) copy-start(bf16[4,1024]{1,0:T(4,128)(2,1)} %param.23) | copy-start | bytes 24580
  26.1 23.0 %copy-start.27 = (bf16[4,1024]{1,0:T(4,128)(2,1)S(1)}, bf16[4,1024]{1,0:T(4,128)(2,1)}, u32[]{:S(2)}) copy-start(bf16[4,1024]{1,0:T(4,128)(2,1)} %param.24) | copy-start | bytes 24580
  27.1 25.3 %copy-start.22 = (bf16[4,2048]{1,0:T(4,128)(2,1)S(1)}, bf16[4,2048]{1,0:T(4,128)(2,1)}, u32[]{:S(2)}) copy-start(bf16[4,2048]{1,0:T(4,128)(2,1)} %param.22) | copy-start | bytes 49156
  57.6 3.9 %copy-start.11 = (bf16[512,256]{1,0:T(8,128)(2,1)S(1)}, bf16[512,256]{1,0:T(8,128)(2,1)}, u32[]{:S(2)}) copy-start(bf16[512,256]{1,0:T(8,128)(2,1)} %copy-done.10) | copy-start | bytes 786436
  59.1 3.1 %copy-start.18 = (f32[1,256]{1,0:T(1,128)S(1)}, f32[1,256]{1,0:T(1,128)}, u32[]{:S(2)}) copy-start(f32[1,256]{1,0:T(1,128)} %get-tuple-element.24) | copy-start | bytes 3076
  59.1 3.2 %copy-start.19 = (f32[1,256]{1,0:T(1,128)S(1)}, f32[1,256]{1,0:T(1,128)}, u32[]{:S(2)}) copy-start(f32[1,256]{1,0:T(1,128)} %get-tuple-element.25) | copy-start | bytes 3076
  59.1 3.2 %copy-start.20 = (f32[1,256]{1,0:T(1,128)S(1)}, f32[1,256]{1,0:T(1,128)}, u32[]{:S(2)}) copy-start(f32[1,256]{1,0:T(1,128)} %get-tuple-element.26) | copy-start | bytes 3076
  59.1 3.2 %copy-start.21 = (f32[1,256]{1,0:T(1,128)S(1)}, f32[1,256]{1,0:T(1,128)}, u32[]{:S(2)}) copy-start(f32[1,256]{1,0:T(1,128)} %get-tuple-element.27) | copy-start | bytes 3076
  61.5 1.3 %copy-start.9 = (bf16[512,512]{1,0:T(8,128)(2,1)S(1)}, bf16[512,512]{1,0:T(8,128)(2,1)}, u32[]{:S(2)}) copy-start(bf16[512,512]{1,0:T(8,128)(2,1)} %copy-done.8) | copy-start | bytes 1572868
  65.0 4.5 %copy-start.1 = (bf16[512,512]{1,0:T(8,128)(2,1)}, bf16[512,512]{1,0:T(8,128)(2,1)S(1)}, u32[]{:S(2)}) copy-start(bf16[512,512]{1,0:T(8,128)(2,1)S(1)} %multiply_convert_fusion.4) | copy-start | bytes 1572868
  66.0 3.5 %copy-start.14 = (f32[2,4]{1,0:T(2,128)S(1)}, f32[2,4]{1,0:T(2,128)}, u32[]{:S(2)}) copy-start(f32[2,4]{1,0:T(2,128)} %get-tuple-element.48) | copy-start | bytes 100
  66.0 3.5 %copy-start.15 = (f32[2,4]{1,0:T(2,128)S(1)}, f32[2,4]{1,0:T(2,128)}, u32[]{:S(2)}) copy-start(f32[2,4]{1,0:T(2,128)} %get-tuple-element.49) | copy-start | bytes 100
  68.0 1.6 %copy-start.16 = (f32[2,4]{1,0:T(2,128)S(1)}, f32[2,4]{1,0:T(2,128)}, u32[]{:S(2)}) copy-start(f32[2,4]{1,0:T(2,128)} %get-tuple-element.50) | copy-start | bytes 100
  68.0 1.6 %copy-start.17 = (f32[2,4]{1,0:T(2,128)S(1)}, f32[2,4]{1,0:T(2,128)}, u32[]{:S(2)}) copy-start(f32[2,4]{1,0:T(2,128)} %get-tuple-element.51) | copy-start | bytes 100
  72.0 10.2 %all-to-all-start = ((f32[4,1,16384]{2,1,0:T(1,128)}), f32[4,1,16384]{2,1,0:T(1,128)S(1)}, u32[]{:S(2)}, u32[]{:S(2)}) async-start(f32[4,1,16384]{2,1,0:T(1,128)} %reshape.274), calls=%async_computation | async-start | bytes 524288 | tf_op jit(solution)/shard_map/all_to_all | solution.py:136
  75.9 9.8 %copy-start.30 = (pred[4,4]{1,0:T(4,128)(4,1)S(1)}, pred[4,4]{1,0:T(4,128)(4,1)}, u32[]{:S(2)}) copy-start(pred[4,4]{1,0:T(4,128)(4,1)} %iota_compare_fusion.1) | copy-start | bytes 52
  84.3 7.2 %copy-start.28 = (f32[2,4]{1,0:T(2,128)S(1)}, f32[2,4]{1,0:T(2,128)}, u32[]{:S(2)}) copy-start(f32[2,4]{1,0:T(2,128)} %mul.529) | copy-start | bytes 100
  84.3 7.4 %copy-start.24 = (bf16[2,32,1,1]{1,0,2,3:T(2,128)(2,1)S(1)}, bf16[2,32,1,1]{1,0,2,3:T(2,128)(2,1)}, u32[]{:S(2)}) copy-start(bf16[2,32,1,1]{1,0,2,3:T(2,128)(2,1)} %fusion.81) | copy-start | bytes 388
  85.7 18.4 %copy-start.29 = (f32[2,4]{1,0:T(2,128)S(1)}, f32[2,4]{1,0:T(2,128)}, u32[]{:S(2)}) copy-start(f32[2,4]{1,0:T(2,128)} %mul.552) | copy-start | bytes 100
  88.1 18.8 %all-to-all-start.1 = ((f32[4,1,16384]{2,1,0:T(1,128)}), f32[4,1,16384]{2,1,0:T(1,128)S(1)}, u32[]{:S(2)}, u32[]{:S(2)}) async-start(f32[4,1,16384]{2,1,0:T(1,128)} %reshape.276), calls=%async_computation.1 | async-start | bytes 524288 | tf_op jit(solution)/shard_map/all_to_all | solution.py:147
  91.5 17.9 %copy-start.31 = (f32[4]{0:T(128)S(1)}, f32[4]{0:T(128)}, u32[]{:S(2)}) copy-start(f32[4]{0:T(128)} %pad.6.clone) | copy-start | bytes 52
  113.5 3.5 %copy-start.2 = (bf16[512,512]{1,0:T(8,128)(2,1)S(1)}, bf16[512,512]{1,0:T(8,128)(2,1)}, u32[]{:S(2)}) copy-start(bf16[512,512]{1,0:T(8,128)(2,1)} %copy-done.1) | copy-start | bytes 1572868
  113.5 3.5 %copy-start.25 = (f32[512]{0:T(512)S(1)}, f32[512]{0:T(512)}, u32[]{:S(2)}) copy-start(f32[512]{0:T(512)} %mul.510) | copy-start | bytes 6148
  124.2 1.2 copy-start.7
where the time goes:
time: 127 us; the launch traced here: 126 us
  blocking collectives  30.3 us (24%)
  local copies, waits for them, and re-layouts  28.8 us (23%)
  matrix products  22.6 us (18%)
  other arithmetic  20.4 us (16%)
  starting transfers between devices  19.8 us (16%)
  waiting for transfers between devices  3.3 us (3%)
    ppermute x3, starting transfers between devices, passed_along(): return lax.ppermute(block, axis, route)  12.8 us
    dot_general x8, matrix products, project(): jnp.dot(operand, weights, preferred_element_type=jnp.float32)  12.6 us
    psum x1, blocking collectives, on_device(): reading = lax.psum(partial_value, 'sp')  12.2 us
    psum x1, blocking collectives, from_root(): return lax.psum(kept, axis)  10.5 us
    all_gather x1, blocking collectives, on_device(): lax.all_gather(shard_fading_factor[None], 'sp', axis=0, tiled=True)  7.58 us
    unnamed x75, local copies, waits for them, and re-layouts  6.63 us
    reshape x2, local copies, waits for them, and re-layouts, on_device(): (inner_part + carried_part).reshape(row_count, head_count, HEAD)  5.28 us
    all_to_all x1, starting transfers between devices, on_device(): lax.all_to_all(running[None], 'sp', split_axis=1, concat_axis=0, tiled=True)  3.58 us
  transfers between devices with their start and end apart: 5, of which 1 were waited for; matrix products, arithmetic and copies ran while one was open for 26% of the time, Pallas kernels for 0%

commit v1 on v0

--- a/solution.py
+++ b/solution.py
@@ -129,7 +129,10 @@
     local_states = jnp.stack(inside)
     shard_fading_factor = jnp.sum(block_end, axis=0)
     before_block = jnp.cumsum(block_end, axis=0) - block_end
-    decay_table = lax.all_gather(shard_fading_factor[None], "sp", axis=0, tiled=True)
+    decay_table = jnp.concatenate(
+        lax.all_to_all(jnp.stack([shard_fading_factor[None]] * lax.axis_size("sp")), "sp", 0, 0),
+        axis=0,
+    )
     inclusive = jnp.cumsum(decay_table, axis=0)
     exclusive = inclusive - decay_table
     total_decay = inclusive[-1]

time: 127 us -> 137 us (1.079)
  blocking collectives: 30.3 us -> 22.2 us
  matrix products: 22.6 us -> 29.1 us
  other arithmetic: 20.4 us -> 24.6 us
  local copies, waits for them, and re-layouts: 28.8 us -> 32.2 us
  starting transfers between devices: 19.8 us -> 23.1 us
    all_gather x1 -> x0, blocking collectives: 7.58 us -> none  [on_device(): lax.all_gather(shard_fading_factor[None], 'sp', axis=0, tiled=True)]
    dot_general x8, matrix products: 12.6 us -> 16.1 us  [project(): jnp.dot(operand, weights, preferred_element_type=jnp.float32)]
    all_to_all x0 -> x1, starting transfers between devices: none -> 3.23 us  [on_device(): lax.all_to_all(jnp.stack([shard_fading_factor[None]] * lax.axis_size('sp'...]
    unnamed x75 -> x45, local copies, waits for them, and re-layouts: 6.63 us -> 6.51 us
  transfers between devices with their start and end apart: 5 -> 6, of which waited for: 1 -> 1; matrix products, arithmetic and copies ran while one was open for 26% -> 33% of each run, Pallas kernels for 0% -> 0%
where the time goes in v1:
time: 137 us; the launch traced here: 136 us
  local copies, waits for them, and re-layouts  32.2 us (24%)
  matrix products  29.1 us (21%)
  other arithmetic  24.6 us (18%)
  starting transfers between devices  23.1 us (17%)
  blocking collectives  22.2 us (16%)
  waiting for transfers between devices  3.35 us (2%)
    dot_general x8, matrix products, project(): jnp.dot(operand, weights, preferred_element_type=jnp.float32)  16.1 us
    ppermute x3, starting transfers between devices, passed_along(): return lax.ppermute(block, axis, route)  12.9 us
    psum x1, blocking collectives, on_device(): reading = lax.psum(partial_value, 'sp')  12.2 us
    psum x1, blocking collectives, from_root(): return lax.psum(kept, axis)  9.99 us
    unnamed x45, local copies, waits for them, and re-layouts  6.51 us
    reshape x2, local copies, waits for them, and re-layouts, on_device(): (inner_part + carried_part).reshape(row_count, head_count, HEAD)  5.33 us
    convert_element_type x5, other arithmetic, apply_taps(): joined = jnp.concatenate([previous, current], axis=0).astype(jnp.float32)  3.62 us
    all_to_all x1, starting transfers between devices, on_device(): lax.all_to_all(running[None], 'sp', split_axis=1, concat_axis=0, tiled=True)  3.58 us
  transfers between devices with their start and end apart: 6, of which 1 were waited for; matrix products, arithmetic and copies ran while one was open for 33% of the time, Pallas kernels for 0%

profile of v1, /device:TPU:0, one launch (start us, length us, event | category | flops | bytes accessed | tf_op | source)
XLA Modules:
  0.0 135.7 jit_solution(11693514717989658256)
XLA Ops:
  0.7 1.6 %copy-done = bf16[512,2048]{1,0:T(8,128)(2,1)S(1)} copy-done((bf16[512,2048]{1,0:T(8,128)(2,1)S(1)}, bf16[512,2048]{1,0:T(8,128)(2,1)}, u32[]{:S(2)}) %copy-start) | copy-done | bytes 2097176
  2.2 1.9 %convolution_convert_fusion.2 = bf16[512,256]{1,0:T(8,128)(2,1)S(1)} fusion(bf16[512,2048]{1,0:T(8,128)(2,1)S(1)} %copy-done, bf16[2048,256]{1,0:T(8,128)(2,1)} %param.18), kind=kOutput, calls=%fused_computation.11 | convolution fusion | flops 537001984 | bytes 3407872 | tf_op jit(solution)/shard_map/dot_general | solution.py:25
  4.8 5.5 %collective-permute-start.2 = (bf16[3,256]{1,0:T(4,128)(2,1)}, bf16[3,256]{1,0:T(4,128)(2,1)}, u32[]{:S(2)}, u32[]{:S(2)}) collective-permute-start(bf16[3,256]{1,0:T(4,128)(2,1)} %get-tuple-element.57), channel_id=1, source_target_pairs={{0,4},{4,8},{8,12},{1,5},{5,9},{9,13},{2,6},{6,10},{10,14},{3,7},{... | collective-permute-start | bytes 4616 | tf_op jit(solution)/shard_map/ppermute | solution.py:16
  11.6 3.5 %collective-permute-start.1 = (bf16[3,256]{1,0:T(4,128)(2,1)}, bf16[3,256]{1,0:T(4,128)(2,1)}, u32[]{:S(2)}, u32[]{:S(2)}) collective-permute-start(bf16[3,256]{1,0:T(4,128)(2,1)} %get-tuple-element.54), channel_id=1, source_target_pairs={{0,4},{4,8},{8,12},{1,5},{5,9},{9,13},{2,6},{6,10},{10,14},{3,7},{... | collective-permute-start | bytes 4616 | tf_op jit(solution)/shard_map/ppermute | solution.py:16
  15.2 0.9 multiply_exponential_fusion
  16.1 1.4 %multiply_subtract_fusion = (f32[512,8]{0,1:T(8,128)S(1)}, f32[512,8]{0,1:T(8,128)S(1)}) fusion(f32[512,8]{0,1:T(8,128)S(1)} %copy-done.8, f32[8]{0:T(128)S(1)} %get-tuple-element.29, f32[8]{0:T(128)S(1)} %dynamic_slice.37, bf16[512,2048]{1,0:T(8,128)(2,1)S(1)} %copy-done, bf16[2048,32]{0,1:T(8,128)(2,1)} %param.21, s32[]{:T(128)S(6)} %select_n.61), kind=kOutput, calls=%fused_computation.98 | convolution fusion | flops 16814080 | bytes 2179140 | tf_op jit(solution)/shard_map/dot_general | solution.py:94
  18.7 3.2 %all-to-all-start.1 = ((f32[4,1,2,4]{3,2,1,0:T(2,128)}), f32[4,1,2,4]{3,2,1,0:T(2,128)S(1)}, u32[]{:S(2)}, u32[]{:S(2)}) async-start(f32[4,1,2,4]{3,2,1,0:T(2,128)} %stack.4), calls=%async_computation.1 | async-start | bytes 8192 | tf_op jit(solution)/shard_map/all_to_all | solution.py:133
  21.9 2.8 %convolution_convert_fusion.1 = bf16[512,512]{1,0:T(8,128)(2,1)S(1)} fusion(bf16[512,2048]{1,0:T(8,128)(2,1)S(1)} %copy-done, bf16[2048,512]{1,0:T(8,128)(2,1)} %param.17), kind=kOutput, calls=%fused_computation.9 | convolution fusion | flops 1074003968 | bytes 4718592 | tf_op jit(solution)/shard_map/dot_general | solution.py:25
  24.8 0.8 copy-done.6
  26.2 3.9 %collective-permute-start = (bf16[3,512]{1,0:T(4,128)(2,1)}, bf16[3,512]{1,0:T(4,128)(2,1)S(1)}, u32[]{:S(2)}, u32[]{:S(2)}) collective-permute-start(bf16[3,512]{1,0:T(4,128)(2,1)} %get-tuple-element.52), channel_id=1, source_target_pairs={{0,4},{4,8},{8,12},{1,5},{5,9},{9,13},{2,6},{6,10},{10,14},{3,7},{... | collective-permute-start | bytes 9224 | tf_op jit(solution)/shard_map/ppermute | solution.py:16
  30.6 1.6 %fusion.99 = f32[1,256]{1,0:T(1,128)S(1)} fusion(bf16[2048,1]{0,1:T(2,128)(2,1)S(1)} %reshape.253, bf16[2048,256]{1,0:T(8,128)(2,1)} %param.18), kind=kOutput, calls=%fused_computation.198 | convolution fusion | flops 1048576 | bytes 1053696 | tf_op jit(solution)/shard_map/dot_general | solution.py:25
  32.2 1.5 %fusion.98 = f32[1,256]{1,0:T(1,128)S(1)} fusion(bf16[2048,1]{0,1:T(2,128)(2,1)S(1)} %reshape.253, bf16[2048,256]{1,0:T(8,128)(2,1)} %param.19), kind=kOutput, calls=%fused_computation.197 | convolution fusion | flops 1048576 | bytes 1053696 | tf_op jit(solution)/shard_map/dot_general | solution.py:25
  38.6 2.5 %fusion.101 = f32[1,512]{1,0:T(1,128)} fusion(bf16[2048,1]{0,1:T(2,128)(2,1)S(1)} %reshape.253, bf16[2048,512]{1,0:T(8,128)(2,1)} %param.20), kind=kOutput, calls=%fused_computation.200 | convolution fusion | flops 2097152 | bytes 2103296 | tf_op jit(solution)/shard_map/dot_general | solution.py:25
  41.6 10.0 %all-reduce = (bf16[3,512]{1,0:T(4,128)(2,1)S(1)}, bf16[3,256]{1,0:T(4,128)(2,1)S(1)}, bf16[3,256]{1,0:T(4,128)(2,1)S(1)}) all-reduce(bf16[3,512]{1,0:T(4,128)(2,1)S(1)} %get-tuple-element.53, bf16[3,256]{1,0:T(4,128)(2,1)S(1)} %get-tuple-element.56, ...), channel_id=1, replica_groups=mesh['grp'=2,'sp'=4,'tp'=4] {'sp'}, use_global_device_ids=true, to_apply=%region_7.8 | all-reduce | flops 3072 | bytes 12288 | tf_op jit(solution)/shard_map/psum | solution.py:21
  53.1 1.5 %convert_reduce_fusion.1 = (bf16[256]{0:T(256)(128)(2,1)S(1)}, f32[1,256]{1,0:T(1,128)}, f32[1,256]{1,0:T(1,128)}, f32[1,256]{1,0:T(1,128)}, f32[1,256]{1,0:T(1,128)}) fusion(f32[4,256]{1,0:T(4,128)S(1)} %get-tuple-element.63, bf16[4,1024]{1,0:T(4,128)(2,1)} %param.24, s32[]{:T(128)S(6)} %select_n.60, s32[]{:T(128)S(6)} %add.243, s32[]{:T(128)S(6)} %add.244, ...), kind=kLoop, calls=%fused_computation.182 | loop fusion | flops 4096 | bytes 10768 | tf_op jit(solution)/shard_map/convert_element_type | solution.py:192
  54.6 1.5 %convert_convert_fusion = (f32[1,256]{1,0:T(1,128)S(1)}, f32[1,256]{1,0:T(1,128)}, f32[1,256]{1,0:T(1,128)}, f32[1,256]{1,0:T(1,128)}, f32[1,256]{1,0:T(1,128)}) fusion(f32[4,256]{1,0:T(4,128)S(1)} %get-tuple-element.64, bf16[4,1024]{1,0:T(4,128)(2,1)} %param.23, s32[]{:T(128)S(6)} %select_n.60, s32[]{:T(128)S(6)} %add.243, s32[]{:T(128)S(6)} %add.244, ...), kind=kLoop, calls=%fused_computation.181 | loop fusion | flops 4352 | bytes 11280 | tf_op jit(solution)/shard_map/reshape | solution.py:194
  56.8 1.5 %fusion.93 = (f32[4,128,2,4]{3,2,1,0:T(2,128)}, f32[4,128,2,4]{3,2,1,0:T(2,128)}) fusion(f32[4,128,2,4]{3,2,1,0:T(2,128)S(1)} %fusion.97, f32[4,128,2,4]{3,2,1,0:T(2,128)S(1)} %copy.152, f32[4,2,4]{2,1,0:T(2,128)S(1)} %get-tuple-element.47), kind=kLoop, calls=%fused_computation.191 | loop fusion | flops 8192 | bytes 65664 | tf_op jit(solution)/shard_map/exp | solution.py:167
  58.4 1.2 copy.151
  59.6 1.3 copy.153
  60.9 1.3 broadcast_multiply_fusion
  64.8 1.0 maximum_convert_fusion.2
  65.9 1.0 multiply_convert_fusion.5
  68.1 1.2 maximum_convert_fusion
  70.0 1.0 copy.143
  71.0 2.0 %reshape.234 = bf16[4,128,2,4,64]{1,0,4,3,2:T(4,128)(2,1)} reshape(bf16[512,512]{0,1:T(8,128)(2,1)} %copy.143) | data formatting | bytes 1048576 | tf_op jit(solution)/shard_map/reshape | solution.py:109
  73.0 1.2 multiply_convert_fusion.3
  74.5 1.0 slice_add_fusion
  75.8 1.2 reshape.276
  76.9 3.6 %all-to-all-start = ((f32[4,1,16384]{2,1,0:T(1,128)}), f32[4,1,16384]{2,1,0:T(1,128)S(1)}, u32[]{:S(2)}, u32[]{:S(2)}) async-start(f32[4,1,16384]{2,1,0:T(1,128)} %reshape.276), calls=%async_computation | async-start | bytes 524288 | tf_op jit(solution)/shard_map/all_to_all | solution.py:139
  80.8 2.9 %convolution_bitcast_fusion.2 = f32[4,128,2,4,64]{1,4,3,2,0:T(8,128)} fusion(f32[4,2,4,128]{3,2,1,0:T(4,128)S(1)} %copy.149, f32[4,2,4,128]{3,2,1,0:T(4,128)S(1)} %copy.147, f32[4,2,128,128]{3,2,1,0:T(8,128)S(1)} %fusion.40, pred[128,128]{1,0:T(8,128)(4,1)S(1)} %iota_compare_fusion, bf16[4,128,2,4,64]{1,0,4,3,2:T(4,128)(2,1)} %reshape.234), kind=kOutput, calls=%fused_computation.5 | convolution fusion | flops 69730304 | bytes 2146304 | tf_op jit(solution)/shard_map/bgels,bsgep->blgep/dot_general | solution.py:163
  83.8 3.3 %all-to-all-done = f32[4,1,16384]{2,1,0:T(1,128)S(1)} async-done(((f32[4,1,16384]{2,1,0:T(1,128)}), f32[4,1,16384]{2,1,0:T(1,128)S(1)}, u32[]{:S(2)}, u32[]{:S(2)}) %all-to-all-start) | async-done | bytes 262176 | tf_op jit(solution)/shard_map/all_to_all | solution.py:139
  87.7 1.4 %reduce.9 = f32[4,16384]{1,0:T(4,128)S(1)} reduce(f32[4,1,16384]{2,1,0:T(1,128)S(1)} %all-to-all-done, f32[]{:T(128)} %broadcast.119), dimensions={1}, to_apply=%all_to_all.8.reduce_sub_computation | reduce | bytes 524292 | tf_op jit(solution)/shard_map/all_to_all | solution.py:139
  89.4 2.0 %fusion.35 = bf16[2,4,1,32,64]{4,2,3,1,0:T(2,128)(2,1)S(1)} fusion(f32[4,2,4,1,1]{0,3,4,2,1:T(1,128)} %copy.177, f32[4,32,2,4,64]{4,3,2,1,0:T(4,128)S(1)} %bitcast.132), kind=kOutput, calls=%fused_computation.69 | convolution fusion | flops 786432 | bytes 295040 | tf_op jit(solution)/shard_map/kge,kngep->ngep/dot_general | solution.py:147
  91.4 2.0 %convolution_bitcast_fusion.3 = f32[4,32,2,4,64]{4,0,1,3,2:T(4,128)S(1)} fusion(f32[4,32,2,4,64]{4,3,2,1,0:T(4,128)S(1)} %bitcast.133, f32[4,2,4]{0,2,1:T(4,128)} %copy.160, f32[4,2,4]{0,2,1:T(4,128)} %copy.159, pred[4,4]{1,0:T(4,128)(4,1)} %iota_compare_fusion.1), kind=kOutput, calls=%fused_computation.10 | convolution fusion | flops 3145984 | bytes 524560 | tf_op jit(solution)/shard_map/jkge,kngep->jngep/dot_general | solution.py:143
  93.5 1.0 reshape.278
  94.6 3.4 %all-to-all-start.2 = ((f32[4,1,16384]{2,1,0:T(1,128)}), f32[4,1,16384]{2,1,0:T(1,128)S(1)}, u32[]{:S(2)}, u32[]{:S(2)}) async-start(f32[4,1,16384]{2,1,0:T(1,128)} %reshape.278), calls=%async_computation.2 | async-start | bytes 524288 | tf_op jit(solution)/shard_map/all_to_all | solution.py:150
  98.0 0.9 bitcast_add_fusion
  98.9 0.8 fusion.43
  99.7 12.2 %psum.31 = f32[2,4,64]{2,1,0:T(4,128)S(1)} all-reduce(f32[2,4,64]{2,1,0:T(4,128)S(1)} %bitcast.146), channel_id=1, replica_groups=mesh['grp'=2,'sp'=4,'tp'=4] {'sp'}, use_global_device_ids=true, to_apply=%region_8.9 | all-reduce | flops 512 | bytes 4096 | tf_op jit(solution)/shard_map/psum | solution.py:203
  114.4 0.8 multiply_convert_fusion.7
  116.0 1.4 %reduce.10 = f32[4,16384]{1,0:T(4,128)S(1)} reduce(f32[4,1,16384]{2,1,0:T(1,128)S(1)} %all-to-all-done.2, f32[]{:T(128)} %broadcast.119), dimensions={1}, to_apply=%all_to_all.22.reduce_sub_computation | reduce | bytes 524292 | tf_op jit(solution)/shard_map/all_to_all | solution.py:150
  117.7 0.9 copy.164
  118.6 2.3 %fusion.1 = f32[4,128,2,4,64]{1,4,3,2,0:T(8,128)S(1)} fusion(f32[4,128,2,4,64]{1,4,3,2,0:T(8,128)} %convolution_bitcast_fusion.2, f32[1,128,2,4,64]{1,4,3,2,0:T(8,128)} %get-tuple-element.41, f32[1,128,2,4,64]{1,4,3,2,0:T(8,128)} %get-tuple-element.42, f32[1,128,2,4,64]{1,4,3,2,0:T(8,128)} %get-tuple-element.43, f32[4]{0:T(128)} %pad.6.clone, ...), kind=kOutput, calls=%fused_computation.4 | convolution fusion | flops 404488192 | bytes 3424400 | tf_op jit(solution)/shard_map/blgn,bngep->blgep/dot_general | solution.py:167
  120.9 1.8 %copy.188 = f32[4,128,2,4,64]{4,3,2,1,0:T(4,128)} copy(f32[4,128,2,4,64]{1,4,3,2,0:T(8,128)S(1)} %fusion.1) | data formatting | bytes 2097152 | tf_op jit(solution)/shard_map/reshape | solution.py:173
  122.8 3.5 %reshape.265 = f32[512,512]{1,0:T(8,128)} reshape(f32[4,128,2,4,64]{4,3,2,1,0:T(4,128)} %copy.188) | data formatting | bytes 2097152 | tf_op jit(solution)/shard_map/reshape | solution.py:173
  126.3 4.6 %fusion.96 = (f32[512,512]{1,0:T(8,128)}, f32[512,512]{1,0:T(8,128)}) fusion(bf16[512,2048]{1,0:T(8,128)(2,1)S(1)} %copy-done, bf16[2048,512]{1,0:T(8,128)(2,1)} %param.20, f32[512,512]{1,0:T(8,128)} %reshape.265, bf16[512,512]{1,0:T(8,128)(2,1)S(1)} %copy-done.2, f32[512]{0:T(512)S(1)} %copy-done.15), kind=kOutput, calls=%fused_computation.194 | convolution fusion | flops 1076625408 | bytes 7866368 | tf_op jit(solution)/shard_map/dot_general | solution.py:25
  130.9 1.9 %mul.516 = f32[512,2,256]{2,1,0:T(2,128)S(1)} reshape(f32[512,512]{1,0:T(8,128)} %get-tuple-element.61) | data formatting | bytes 2097152 | tf_op jit(solution)/shard_map/mul | solution.py:39
  134.6 1.1 multiply_convert_fusion.2
  (117 shorter events, 23.7 us)
Async XLA Ops:
  0.6 1.6 %copy-start = (bf16[512,2048]{1,0:T(8,128)(2,1)S(1)}, bf16[512,2048]{1,0:T(8,128)(2,1)}, u32[]{:S(2)}) copy-start(bf16[512,2048]{1,0:T(8,128)(2,1)} %param.15) | copy-start | bytes 6291460
  0.6 9.7 %copy-start.4 = (bf16[2048,256]{1,0:T(8,128)(2,1)S(1)}, bf16[2048,256]{1,0:T(8,128)(2,1)}, u32[]{:S(2)}) copy-start(bf16[2048,256]{1,0:T(8,128)(2,1)} %param.19) | copy-start | bytes 3145732
  4.2 6.9 %copy-start.7 = (bf16[512,256]{1,0:T(8,128)(2,1)}, bf16[512,256]{1,0:T(8,128)(2,1)S(1)}, u32[]{:S(2)}) copy-start(bf16[512,256]{1,0:T(8,128)(2,1)S(1)} %convolution_convert_fusion.2) | copy-start | bytes 786436
  4.2 10.9 %copy-start.14 = (bf16[2048]{0:T(1024)(128)(2,1)S(1)}, bf16[2048]{0:T(1024)(128)(2,1)}, u32[]{:S(2)}) copy-start(bf16[2048]{0:T(1024)(128)(2,1)} %param.16) | copy-start | bytes 12292
  4.2 10.9 %copy-start.17 = (f32[32]{0:T(128)S(1)}, f32[32]{0:T(128)}, u32[]{:S(2)}) copy-start(f32[32]{0:T(128)} %param.26) | copy-start | bytes 388
  4.2 11.0 %copy-start.16 = (f32[32]{0:T(128)S(1)}, f32[32]{0:T(128)}, u32[]{:S(2)}) copy-start(f32[32]{0:T(128)} %param.25) | copy-start | bytes 388
  4.2 11.9 %copy-start.8 = (f32[512,8]{0,1:T(8,128)S(1)}, f32[512,8]{0,1:T(8,128)}, u32[]{:S(2)}) copy-start(f32[512,8]{0,1:T(8,128)} %param.27) | copy-start | bytes 49156
  4.8 60.0 %collective-permute-start.2 = (bf16[3,256]{1,0:T(4,128)(2,1)}, bf16[3,256]{1,0:T(4,128)(2,1)}, u32[]{:S(2)}, u32[]{:S(2)}) collective-permute-start(bf16[3,256]{1,0:T(4,128)(2,1)} %get-tuple-element.57), channel_id=1, source_target_pairs={{0,4},{4,8},{8,12},{1,5},{5,9},{9,13},{2,6},{6,10},{10,14},{3,7},{... | collective-permute-start | bytes 4616 | tf_op jit(solution)/shard_map/ppermute | solution.py:16
  11.6 55.3 %collective-permute-start.1 = (bf16[3,256]{1,0:T(4,128)(2,1)}, bf16[3,256]{1,0:T(4,128)(2,1)}, u32[]{:S(2)}, u32[]{:S(2)}) collective-permute-start(bf16[3,256]{1,0:T(4,128)(2,1)} %get-tuple-element.54), channel_id=1, source_target_pairs={{0,4},{4,8},{8,12},{1,5},{5,9},{9,13},{2,6},{6,10},{10,14},{3,7},{... | collective-permute-start | bytes 4616 | tf_op jit(solution)/shard_map/ppermute | solution.py:16
  18.7 44.1 %all-to-all-start.1 = ((f32[4,1,2,4]{3,2,1,0:T(2,128)}), f32[4,1,2,4]{3,2,1,0:T(2,128)S(1)}, u32[]{:S(2)}, u32[]{:S(2)}) async-start(f32[4,1,2,4]{3,2,1,0:T(2,128)} %stack.4), calls=%async_computation.1 | async-start | bytes 8192 | tf_op jit(solution)/shard_map/all_to_all | solution.py:133
  24.8 0.8 copy-start.6
  26.2 42.0 %collective-permute-start = (bf16[3,512]{1,0:T(4,128)(2,1)}, bf16[3,512]{1,0:T(4,128)(2,1)S(1)}, u32[]{:S(2)}, u32[]{:S(2)}) collective-permute-start(bf16[3,512]{1,0:T(4,128)(2,1)} %get-tuple-element.52), channel_id=1, source_target_pairs={{0,4},{4,8},{8,12},{1,5},{5,9},{9,13},{2,6},{6,10},{10,14},{3,7},{... | collective-permute-start | bytes 9224 | tf_op jit(solution)/shard_map/ppermute | solution.py:16
  30.1 3.6 %copy-start.3 = (bf16[2048,512]{1,0:T(8,128)(2,1)S(1)}, bf16[2048,512]{1,0:T(8,128)(2,1)}, u32[]{:S(2)}) copy-start(bf16[2048,512]{1,0:T(8,128)(2,1)} %param.17) | copy-start | bytes 6291460
  30.6 4.1 %copy-start.18 = (f32[32]{0:T(128)S(1)}, f32[32]{0:T(128)}, u32[]{:S(2)}) copy-start(f32[32]{0:T(128)} %param.28) | copy-start | bytes 388
  34.0 17.6 %copy-start.13 = (bf16[4,2048]{1,0:T(4,128)(2,1)S(1)}, bf16[4,2048]{1,0:T(4,128)(2,1)}, u32[]{:S(2)}) copy-start(bf16[4,2048]{1,0:T(4,128)(2,1)} %param.22) | copy-start | bytes 49156
  60.8 6.8 %copy-start.9 = (f32[1,256]{1,0:T(1,128)S(1)}, f32[1,256]{1,0:T(1,128)}, u32[]{:S(2)}) copy-start(f32[1,256]{1,0:T(1,128)} %get-tuple-element.24) | copy-start | bytes 3076
  60.8 6.8 %copy-start.10 = (f32[1,256]{1,0:T(1,128)S(1)}, f32[1,256]{1,0:T(1,128)}, u32[]{:S(2)}) copy-start(f32[1,256]{1,0:T(1,128)} %get-tuple-element.25) | copy-start | bytes 3076
  60.8 6.8 %copy-start.11 = (f32[1,256]{1,0:T(1,128)S(1)}, f32[1,256]{1,0:T(1,128)}, u32[]{:S(2)}) copy-start(f32[1,256]{1,0:T(1,128)} %get-tuple-element.26) | copy-start | bytes 3076
  60.8 6.8 %copy-start.12 = (f32[1,256]{1,0:T(1,128)S(1)}, f32[1,256]{1,0:T(1,128)}, u32[]{:S(2)}) copy-start(f32[1,256]{1,0:T(1,128)} %get-tuple-element.27) | copy-start | bytes 3076
  70.0 4.5 %copy-start.1 = (bf16[512,512]{1,0:T(8,128)(2,1)}, bf16[512,512]{1,0:T(8,128)(2,1)S(1)}, u32[]{:S(2)}) copy-start(bf16[512,512]{1,0:T(8,128)(2,1)S(1)} %multiply_convert_fusion.4) | copy-start | bytes 1572868
  76.9 10.2 %all-to-all-start = ((f32[4,1,16384]{2,1,0:T(1,128)}), f32[4,1,16384]{2,1,0:T(1,128)S(1)}, u32[]{:S(2)}, u32[]{:S(2)}) async-start(f32[4,1,16384]{2,1,0:T(1,128)} %reshape.276), calls=%async_computation | async-start | bytes 524288 | tf_op jit(solution)/shard_map/all_to_all | solution.py:139
  94.6 21.4 %all-to-all-start.2 = ((f32[4,1,16384]{2,1,0:T(1,128)}), f32[4,1,16384]{2,1,0:T(1,128)S(1)}, u32[]{:S(2)}, u32[]{:S(2)}) async-start(f32[4,1,16384]{2,1,0:T(1,128)} %reshape.278), calls=%async_computation.2 | async-start | bytes 524288 | tf_op jit(solution)/shard_map/all_to_all | solution.py:150
  122.7 3.5 %copy-start.2 = (bf16[512,512]{1,0:T(8,128)(2,1)S(1)}, bf16[512,512]{1,0:T(8,128)(2,1)}, u32[]{:S(2)}) copy-start(bf16[512,512]{1,0:T(8,128)(2,1)} %copy-done.1) | copy-start | bytes 1572868
  122.8 3.5 %copy-start.15 = (f32[512]{0:T(512)S(1)}, f32[512]{0:T(512)}, u32[]{:S(2)}) copy-start(f32[512]{0:T(512)} %mul.510) | copy-start | bytes 6148
  133.4 1.2 copy-start.5
